TPU v7x, 32 devices: a whole 2x2x4 slice. The times are simulated.
32 devices in a mesh: ep: 16 (over z, y, x), tp: 2 (over core).
Axes of the slice: x: 2, y: 2, z: 4, core: 2. Of those that a mesh axis runs over, the one named last changes fastest.
Arguments:
- tokens: bfloat16 [512, 1024], P(('ep', 'tp')), may hold values from -6 to 6
- lengths: int32 [512], P(('ep', 'tp')), may hold values from 1 to 1024
- cache_latent: bfloat16 [512, 1024, 256], P(('ep', 'tp')), may hold values from -700 to 700
- cache_rope: bfloat16 [512, 32, 1024], P(('ep', 'tp')), may hold values from -6 to 6
- attn_gain: bfloat16 [1024], replicated, may hold values from 0.099609375 to 1.8984375
- w_dq: bfloat16 [1024, 512], replicated, may hold values from -0.1875 to 0.1875
- q_gain: bfloat16 [512], replicated, may hold values from 0.099609375 to 1.8984375
- w_q_nope: bfloat16 [512, 1024], replicated, may hold values from -0.25 to 0.25
- w_q_rope: bfloat16 [512, 512], replicated, may hold values from -0.25 to 0.25
- w_dkv: bfloat16 [1024, 256], replicated, may hold values from -0.1875 to 0.1875
- kv_gain: bfloat16 [256], replicated, may hold values from 0.099609375 to 1.8984375
- w_krope: bfloat16 [1024, 32], replicated, may hold values from -0.1875 to 0.1875
- w_uk: bfloat16 [256, 1024], replicated, may hold values from -0.75 to 0.75
- w_uv: bfloat16 [256, 1024], replicated, may hold values from -0.375 to 0.375
- w_o: bfloat16 [1024, 1024], replicated, may hold values from -0.1875 to 0.1875
- post_gain: bfloat16 [1024], replicated, may hold values from 0.099609375 to 1.8984375
- moe_gain: bfloat16 [1024], replicated, may hold values from 0.099609375 to 1.8984375
- routes: int32 [512, 4], P(('ep', 'tp')), may hold values from 0 to 15, all different within a row; in each aligned block of 16 rows (0 to 15, 16 to 31, ...) at most 6 rows name the same one
- route_scores: float32 [512, 4], P(('ep', 'tp')), may hold values from 0.05 to 1
- expert_gate: bfloat16 [16, 1024, 512], P('ep', None, 'tp'), may hold values from -0.1875 to 0.1875
- expert_up: bfloat16 [16, 1024, 512], P('ep', None, 'tp'), may hold values from -0.1875 to 0.1875
- expert_down: bfloat16 [16, 512, 1024], P('ep', 'tp'), may hold values from -0.25 to 0.25
- shared_gate: bfloat16 [1024, 512], replicated, may hold values from -0.1875 to 0.1875
- shared_up: bfloat16 [1024, 512], replicated, may hold values from -0.1875 to 0.1875
- shared_down: bfloat16 [512, 1024], replicated, may hold values from -0.25 to 0.25
- dense_vec: bfloat16 [1024], replicated, may hold values from -0.1875 to 0.1875
- dense_w_gate: bfloat16 [1024, 8192], P(None, ('ep', 'tp')), may hold values from -0.1875 to 0.1875
- dense_w_up: bfloat16 [1024, 8192], P(None, ('ep', 'tp')), may hold values from -0.1875 to 0.1875
- dense_w_down: bfloat16 [8192, 1024], P(('ep', 'tp')), may hold values from -0.125 to 0.125
- out_gain: bfloat16 [1024], replicated, may hold values from 0.099609375 to 1.8984375
Outputs:
- hidden_out: bfloat16 [512, 1024], P(('ep', 'tp'))
- new_latent: bfloat16 [512, 256], P(('ep', 'tp'))
Inputs may be any that keep to these rules, and one draw needn't show every extreme that they name: `routes`: each row names 4 different experts. In the 16 rows of one device no expert is named more than 6 times, a bound that some block reaches in some devices' rows.
All inputs are finite; a program needn't handle non-finite values.
Results may differ from a plain program's by a relative error of at most 0.011.
The roundings to bfloat16 on the way count: a program that leaves them out, or rounds other values in their place, can miss the bound.
Values may be sent and summed in bfloat16 or wider, within the bound.
A program may use at most 128 MiB of HBM per device.

v0:
```python
import jax
import jax.numpy as jnp
from jax import lax
from jax.sharding import PartitionSpec as P

HEADS = 16
NOPE = 64
ROPE = 32
VDIM = 64


eps = 1e-06
rope_base = 10000.0
routed_scale = 2.5


def rms_scale(value, gain):
    value = value.astype(jnp.float32)
    inverse = lax.rsqrt(jnp.mean(value * value, axis=-1, keepdims=True) + eps)
    return value * inverse * gain.astype(jnp.float32)


def angles(lengths, rope_dim):
    half = rope_dim // 2
    freqs = rope_base ** (-jnp.arange(half, dtype=jnp.float32) / half)
    angle = lengths.astype(jnp.float32)[:, None] * freqs[None, :]
    return (jnp.cos(angle), jnp.sin(angle))


def rotate(value, cosine, sine):
    half = value.shape[-1] // 2
    first, second = (value[..., :half], value[..., half:])
    return jnp.concatenate(
        [first * cosine - second * sine, second * cosine + first * sine], axis=-1
    )


def slot_table(ids, scores, experts, cap):
    rows, top = ids.shape
    norm = scores / jnp.sum(scores, axis=1, keepdims=True) * routed_scale
    flat = ids.reshape(-1)
    onehot = (flat[:, None] == jnp.arange(experts, dtype=jnp.int32)[None, :]).astype(jnp.int32)
    rank = jnp.cumsum(onehot, axis=0) - 1
    hit = onehot[:, :, None] * (
        rank[:, :, None] == jnp.arange(cap, dtype=jnp.int32)[None, None, :]
    ).astype(jnp.int32)
    owner = jnp.arange(rows * top, dtype=jnp.int32) // top
    token_of = jnp.sum(hit * owner[:, None, None], axis=0)
    weight_of = jnp.sum(hit.astype(jnp.float32) * norm.reshape(-1)[:, None, None], axis=0)
    return (token_of, weight_of)


def attention(
    tokens,
    lengths,
    latent,
    rope_keys,
    attn_gain,
    w_dq,
    q_gain,
    w_q_nope,
    w_q_rope,
    w_dkv,
    kv_gain,
    w_krope,
    w_uk,
    w_uv,
    w_o,
    post_gain,
):
    f32 = jnp.float32
    bf16 = jnp.bfloat16
    seqs = tokens.shape[0]
    latent_width = w_dkv.shape[1]
    normed = rms_scale(tokens, attn_gain).astype(bf16)
    q_normed = rms_scale(jnp.dot(normed, w_dq, preferred_element_type=f32), q_gain).astype(bf16)
    q_nope = (
        jnp.dot(q_normed, w_q_nope, preferred_element_type=f32)
        .astype(bf16)
        .reshape(seqs, HEADS, NOPE)
    )
    cosine, sine = angles(lengths, ROPE)
    q_raw = jnp.dot(q_normed, w_q_rope, preferred_element_type=f32).reshape(seqs, HEADS, ROPE)
    q_rot = rotate(q_raw, cosine[:, None, :], sine[:, None, :]).astype(bf16)
    new_latent = rms_scale(jnp.dot(normed, w_dkv, preferred_element_type=f32), kv_gain).astype(bf16)
    new_rope = rotate(jnp.dot(normed, w_krope, preferred_element_type=f32), cosine, sine).astype(
        bf16
    )
    query_lat = jnp.einsum(
        "shn,chn->shc", q_nope, w_uk.reshape(latent_width, HEADS, NOPE), preferred_element_type=f32
    ).astype(bf16)
    scale = (NOPE + ROPE) ** (-0.5)
    past = jnp.einsum("shc,slc->shl", query_lat, latent, preferred_element_type=f32)
    past = (past + jnp.einsum("shr,srl->shl", q_rot, rope_keys, preferred_element_type=f32)) * scale
    own = jnp.einsum("shc,sc->sh", query_lat, new_latent, preferred_element_type=f32)
    own = (own + jnp.einsum("shr,sr->sh", q_rot, new_rope, preferred_element_type=f32)) * scale
    valid = jnp.arange(latent.shape[1], dtype=jnp.int32)[None, None, :] < lengths[:, None, None]
    top = jnp.maximum(jnp.max(jnp.where(valid, past, -1e30), axis=-1), own)
    past_weight = jnp.where(valid, jnp.exp(past - top[..., None]), 0.0)
    own_weight = jnp.exp(own - top)
    total = jnp.sum(past_weight, axis=-1) + own_weight
    past_prob = (past_weight / total[..., None]).astype(bf16)
    own_prob = (own_weight / total).astype(bf16)
    mixed = jnp.einsum("shl,slc->shc", past_prob, latent, preferred_element_type=f32)
    mixed = (mixed + own_prob.astype(f32)[..., None] * new_latent.astype(f32)[:, None, :]).astype(
        bf16
    )
    head_out = jnp.einsum(
        "shc,chv->shv", mixed, w_uv.reshape(latent_width, HEADS, VDIM), preferred_element_type=f32
    ).astype(bf16)
    attn_out = jnp.dot(head_out.reshape(seqs, HEADS * VDIM), w_o, preferred_element_type=f32)
    first = (tokens.astype(f32) + rms_scale(attn_out, post_gain)).astype(bf16)
    return (first, new_latent)


def expert_apply(rows, gate_w, up_w, down_w):
    hidden_gate = jnp.einsum("necd,edf->necf", rows, gate_w, preferred_element_type=jnp.float32)
    hidden_up = jnp.einsum("necd,edf->necf", rows, up_w, preferred_element_type=jnp.float32)
    act = (jax.nn.silu(hidden_gate) * hidden_up).astype(jnp.bfloat16)
    return (
        jnp.einsum("necf,efd->necd", act, down_w, preferred_element_type=jnp.float32)
        .astype(jnp.bfloat16)
        .astype(jnp.float32)
    )


def dense_partial(rows, w_gate, w_up, w_down):
    act = (
        jax.nn.silu(jnp.dot(rows, w_gate, preferred_element_type=jnp.float32))
        * jnp.dot(rows, w_up, preferred_element_type=jnp.float32)
    ).astype(jnp.bfloat16)
    return jnp.dot(act, w_down, preferred_element_type=jnp.float32)


def shards(
    tokens,
    lengths,
    cache_latent,
    cache_rope,
    attn_gain,
    w_dq,
    q_gain,
    w_q_nope,
    w_q_rope,
    w_dkv,
    kv_gain,
    w_krope,
    w_uk,
    w_uv,
    w_o,
    post_gain,
    moe_gain,
    routes,
    route_scores,
    expert_gate,
    expert_up,
    expert_down,
    shared_gate,
    shared_up,
    shared_down,
    dense_vec,
    dense_w_gate,
    dense_w_up,
    dense_w_down,
    out_gain,
):
    f32 = jnp.float32
    bf16 = jnp.bfloat16
    first, new_latent = attention(
        tokens,
        lengths,
        cache_latent,
        cache_rope,
        attn_gain,
        w_dq,
        q_gain,
        w_q_nope,
        w_q_rope,
        w_dkv,
        kv_gain,
        w_krope,
        w_uk,
        w_uv,
        w_o,
        post_gain,
    )
    moe_in = rms_scale(first, moe_gain).astype(bf16)
    seqs, width = moe_in.shape
    shared_act = (
        jax.nn.silu(jnp.dot(moe_in, shared_gate, preferred_element_type=f32))
        * jnp.dot(moe_in, shared_up, preferred_element_type=f32)
    ).astype(bf16)
    shared_out = jnp.dot(shared_act, shared_down, preferred_element_type=f32)
    ep_count = lax.axis_size("ep")
    exp_dev = expert_gate.shape[0]
    experts = exp_dev * ep_count
    top = routes.shape[1]
    cap = seqs * top // experts + 2
    token_of, weight_of = slot_table(routes, route_scores, experts, cap)
    outgoing = moe_in[token_of].reshape(ep_count, exp_dev, cap, width)
    arrived = lax.all_to_all(outgoing, "ep", split_axis=0, concat_axis=0, tiled=True)
    pooled = lax.all_gather(arrived, "tp", axis=0, tiled=True)
    partial_out = expert_apply(pooled, expert_gate, expert_up, expert_down)
    summed = lax.psum_scatter(
        partial_out.astype(jnp.bfloat16), "tp", scatter_dimension=0, tiled=True
    ).astype(jnp.float32)
    returned = lax.all_to_all(
        summed.astype(jnp.bfloat16), "ep", split_axis=0, concat_axis=0, tiled=True
    ).astype(summed.dtype)
    match = (token_of.reshape(-1)[None, :] == jnp.arange(seqs, dtype=jnp.int32)[:, None]).astype(
        f32
    ) * weight_of.reshape(-1)[None, :]
    routed = jnp.dot(match, returned.reshape(experts * cap, width), precision=lax.Precision.HIGHEST)
    gate = jax.nn.sigmoid(jnp.dot(moe_in, dense_vec, preferred_element_type=f32))
    rows_side = lax.all_gather(moe_in, "ep", axis=0, tiled=True)
    chip_gate, chip_up = (
        lax.all_gather(dense_w_gate, "tp", axis=1, tiled=True),
        lax.all_gather(dense_w_up, "tp", axis=1, tiled=True),
    )
    chip_down = lax.all_gather(dense_w_down, "tp", axis=0, tiled=True)
    dense_out = lax.psum_scatter(
        dense_partial(rows_side, chip_gate, chip_up, chip_down),
        "ep",
        scatter_dimension=0,
        tiled=True,
    )
    mixture = routed + shared_out + gate[:, None] * dense_out
    hidden_out = (first.astype(f32) + rms_scale(mixture, out_gain)).astype(bf16)
    return (hidden_out, new_latent)


def solution(mesh):
    return jax.shard_map(
        shards,
        mesh=mesh,
        in_specs=(
            P(("ep", "tp"), None),
            P(("ep", "tp")),
            P(("ep", "tp"), None, None),
            P(("ep", "tp"), None, None),
            P(),
            P(),
            P(),
            P(),
            P(),
            P(),
            P(),
            P(),
            P(),
            P(),
            P(),
            P(),
            P(),
            P(("ep", "tp"), None),
            P(("ep", "tp"), None),
            P("ep", None, "tp"),
            P("ep", None, "tp"),
            P("ep", "tp", None),
            P(),
            P(),
            P(),
            P(),
            P(None, ("ep", "tp")),
            P(None, ("ep", "tp")),
            P(("ep", "tp"), None),
            P(),
        ),
        out_specs=(P(("ep", "tp"), None), P(("ep", "tp"), None)),
        check_vma=False,
    )
```

profile of v0, /device:TPU:0, one launch (start us, length us, event | category | flops | bytes accessed | tf_op | source)
XLA Modules:
  0.0 191.2 jit_solution(1836097313410984949)
XLA Ops:
  7.2 0.7 all-gather.4.cloned.1.call-update
  8.0 0.7 all-gather.8.cloned.1.call-update
  8.7 0.7 all-gather.6.cloned.1.call-update
  9.5 0.7 iota_compare_fusion
  10.2 0.7 convert_element_type.129
  10.9 0.7 convert_element_type.139
  11.5 1.2 copy.69
  12.8 0.7 convert_element_type.122
  13.5 0.9 fusion.44
  14.4 0.7 convert_element_type.124
  15.1 1.6 multiply_reduce_fusion.2
  16.7 1.3 fusion.82
  18.0 0.1 reshape.261
  18.1 1.1 fusion.83
  19.1 1.3 copy.66
  20.4 1.5 convolution_convert_fusion.3
  22.0 0.1 reshape.259
  22.1 0.8 convert_element_type.130
  22.9 1.6 multiply_reduce_fusion.3
  24.5 0.1 subtract_convert_fusion.1
  24.6 0.1 maximum_bitcast_fusion
  24.7 0.1 subtract_convert_fusion
  24.8 1.6 fusion.65
  26.4 0.2 fusion.64
  26.6 0.2 fusion.7
  26.9 0.2 fusion.40
  27.0 6.1 %select_reduce_fusion = (f32[16,16]{1,0:T(8,128)S(1)}, f32[16,16,1024]{2,1,0:T(8,128)S(1)}) fusion(pred[16,1024]{1,0:T(8,128)(4,1)S(1)} %iota_compare_fusion, f32[16,16,1024]{2,1,0:T(8,128)S(1)} %fusion.65, bf16[16,1024,256]{2,1,0:T(8,128)(2,1)} %param.32, bf16[16,16,256]{2,0,1:T(8,128)(2,1)S(1)} %fusion.7), kind=kOutput, calls=%fused_computation.31 | convolution fusion | flops 135266048 | bytes 10634240 | tf_op jit(solution)/shard_map/shc,slc->shl/dot_general | solution.py:93
  33.2 0.4 fusion.16
  33.6 1.3 fusion.5
  34.9 0.3 fusion.9
  35.2 0.1 reshape.263
  35.3 0.5 multiply_reduce_fusion.1
  35.9 0.2 fusion.48
  36.1 0.1 copy.72
  36.2 0.1 eq.51
  36.4 0.1 reduce_window_sum.11
  36.6 0.2 fusion.53
  36.8 0.1 copy.78
  36.9 0.1 reshape.273
  37.1 0.8 gather_fusion
  37.9 18.2 %all_to_all.10 = bf16[16,1,6,1024]{3,2,1,0:T(8,128)(2,1)S(1)} all-to-all(bf16[16,1,6,1024]{3,2,1,0:T(8,128)(2,1)S(1)} %bitcast.106), channel_id=1, replica_groups=mesh['ep'=16,'tp'=2] {'ep'}, dimensions={0} | all-to-all | bytes 393216 | tf_op jit(solution)/shard_map/all_to_all | solution.py:201
  56.2 0.1 copy.80
  56.3 2.1 %all_gather.15 = bf16[32,1,6,1024]{3,0,2,1:T(8,128)(2,1)S(1)} all-gather(bf16[16,1,6,1024]{3,0,2,1:T(8,128)(2,1)S(1)} %copy.80), channel_id=1, replica_groups=mesh['ep'=16,'tp'=2] {'tp'}, dimensions={0}, use_global_device_ids=true | all-gather | bytes 589824 | tf_op jit(solution)/shard_map/all_gather | solution.py:202
  58.4 0.3 convolution_bitcast_fusion.1
  58.6 2.6 %fusion.2 = bf16[32,1,6,1024]{3,0,2,1:T(8,128)(2,1)} fusion(bf16[1,256,1024]{2,1,0:T(8,128)(2,1)} %param.51, bf16[1,1024,256]{2,1,0:T(8,128)(2,1)} %param.50, bf16[32,1,6,1024]{3,0,2,1:T(8,128)(2,1)S(1)} %all_gather.15, f32[32,1,6,256]{3,0,2,1:T(8,128)S(1)} %convolution_bitcast_fusion.1), kind=kOutput, calls=%fused_computation.6 | convolution fusion | flops 201818112 | bytes 2031616 | tf_op jit(solution)/shard_map/necf,efd->necd/dot_general | solution.py:121
  61.3 40.8 %all_gather.16 = bf16[256,1024]{1,0:T(8,128)(2,1)S(1)} all-gather(bf16[16,1024]{1,0:T(8,128)(2,1)S(1)} %fusion.50), channel_id=1, replica_groups=mesh['ep'=16,'tp'=2] {'ep'}, dimensions={0}, use_global_device_ids=true | all-gather | bytes 557056 | tf_op jit(solution)/shard_map/all_gather | solution.py:215
  102.1 1.7 fusion.92
  103.8 3.3 %fusion.3 = f32[256,1024]{1,0:T(8,128)} fusion(bf16[512,1024]{1,0:T(8,128)(2,1)} %all-gather.8.cloned.1.call-done, bf16[256,1024]{1,0:T(8,128)(2,1)S(1)} %all_gather.16, bf16[1024,512]{1,0:T(8,128)(2,1)} %all-gather.6.cloned.1.call-done, f32[256,512]{1,0:T(8,128)S(1)} %fusion.92), kind=kOutput, calls=%fused_computation.7 | convolution fusion | flops 537657344 | bytes 4194304 | tf_op jit(solution)/shard_map/dot_general | solution.py:132
  107.2 0.1 copy.75
  107.3 0.1 copy.76
  107.4 0.1 mul.316
  107.5 0.1 fusion.55
  107.6 0.1 copy.77
  107.7 0.1 mul.319
  107.8 0.1 eq.58
  107.9 1.8 copy.81
  109.7 3.5 %all-to-all-start.1 = ((bf16[16,1,6,1024]{3,2,1,0:T(8,128)(2,1)}), bf16[16,1,6,1024]{3,2,1,0:T(8,128)(2,1)S(1)}, u32[]{:S(2)}, u32[]{:S(2)}) async-start(bf16[16,1,6,1024]{3,2,1,0:T(8,128)(2,1)} %copy.81), calls=%async_computation.2 | async-start | bytes 524288 | tf_op jit(solution)/shard_map/all_to_all | solution.py:207
  113.2 0.1 fusion.15
  113.3 1.5 fusion.91
  114.8 6.9 %all-to-all-done.1 = bf16[16,1,6,1024]{3,2,1,0:T(8,128)(2,1)S(1)} async-done(((bf16[16,1,6,1024]{3,2,1,0:T(8,128)(2,1)}), bf16[16,1,6,1024]{3,2,1,0:T(8,128)(2,1)S(1)}, u32[]{:S(2)}, u32[]{:S(2)}) %all-to-all-start.1) | async-done | bytes 196640 | tf_op jit(solution)/shard_map/all_to_all | solution.py:207
  121.7 0.2 fusion.67
  121.9 59.9 %reduce-scatter.5.cloned.1.call-done = f32[16,1024]{1,0:T(8,128)} async-done(((f32[256,1024]{1,0:T(8,128)}), f32[16,1024]{1,0:T(8,128)}) %reduce-scatter.5.cloned.1.call-update) | async-done | bytes 65552 | tf_op jit(solution)/shard_map/reduce_scatter | solution.py:221
  181.9 2.1 %multiply_reduce_fusion = (f32[16]{0:T(128)S(1)}, f32[16,1024]{1,0:T(8,128)S(1)}) fusion(f32[16,1024]{1,0:T(8,128)} %reduce-scatter.5.cloned.1.call-done, f32[16]{0:T(128)S(1)} %fusion.15, f32[16,1024]{1,0:T(8,128)S(1)} %fusion.67, bf16[512,1024]{1,0:T(8,128)(2,1)} %param.54, bf16[16,1024]{1,0:T(8,128)(2,1)S(1)} %fusion.50, bf16[1024,512]{1,0:T(8,128)(2,1)} %param.53, ...), kind=kOutput, calls=%fused_computation.76 | convolution fusion | flops 33685488 | bytes 2359424 | tf_op jit(solution)/shard_map/dot_general | solution.py:193
  184.0 0.7 fusion.51
  (60 shorter events, 1.0 us)
Async XLA Ops:
  7.2 28.2 %copy-start = (bf16[1024,1024]{1,0:T(8,128)(2,1)S(1)}, bf16[1024,1024]{1,0:T(8,128)(2,1)}, u32[]{:S(2)}) copy-start(bf16[1024,1024]{1,0:T(8,128)(2,1)} %param.44) | copy-start | bytes 6291460
  7.2 94.9 %all-gather.4.cloned.1.call-start = ((), (), s32[]{:S(2)}) async-start(), calls=%async_computation.5 | async-start | bytes 1572864 | tf_op jit(solution)/shard_map/all_gather | solution.py:217
  7.9 95.9 %all-gather.8.cloned.1.call-start = ((), (), s32[]{:S(2)}) async-start(), calls=%async_computation.7 | async-start | bytes 1572864 | tf_op jit(solution)/shard_map/all_gather | solution.py:220
  8.7 95.1 %all-gather.6.cloned.1.call-start = ((), (), s32[]{:S(2)}) async-start(), calls=%async_computation.6 | async-start | bytes 1572864 | tf_op jit(solution)/shard_map/all_gather | solution.py:218
  9.4 98.5 %reduce-scatter.3.cloned.1.call-start = ((), (), s32[]{:S(2)}) async-start(), calls=%async_computation.4 | async-start | bytes 589824 | tf_op jit(solution)/shard_map/reduce_scatter | solution.py:204
  22.1 11.5 %slice-start = ((s8[8388608]{0:T(1024)(128)(4,1)}), s8[4194304]{0:T(1024)(128)(4,1)S(1)}, s32[]{:S(2)}) async-start(s8[8388608]{0:T(1024)(128)(4,1)} %bitcast.102), calls=%async_computation.9 | async-start | bytes 8388608
  26.9 8.0 %copy-start.4 = (bf16[16,256]{1,0:T(8,128)(2,1)}, bf16[16,256]{1,0:T(8,128)(2,1)S(1)}, u32[]{:S(2)}) copy-start(bf16[16,256]{1,0:T(8,128)(2,1)S(1)} %get-tuple-element.5) | copy-start | bytes 24580
  27.0 6.5 %slice-start.1 = ((s8[8388608]{0:T(1024)(128)(4,1)}), s8[4194304]{0:T(1024)(128)(4,1)S(1)}, s32[]{:S(2)}) async-start(s8[8388608]{0:T(1024)(128)(4,1)} %bitcast.102), calls=%async_computation.10 | async-start | bytes 8388608
  33.6 2.3 %copy-start.5 = (bf16[1024]{0:T(1024)(128)(2,1)S(1)}, bf16[1024]{0:T(1024)(128)(2,1)}, u32[]{:S(2)}) copy-start(bf16[1024]{0:T(1024)(128)(2,1)} %param.46) | copy-start | bytes 6148
  33.6 2.3 %copy-start.1 = (bf16[16,1024]{1,0:T(8,128)(2,1)S(1)}, bf16[16,1024]{1,0:T(8,128)(2,1)}, u32[]{:S(2)}) copy-start(bf16[16,1024]{1,0:T(8,128)(2,1)} %param.30) | copy-start | bytes 98308
  33.6 2.5 %copy-start.6 = (s32[16,4]{0,1:T(4,128)S(1)}, s32[16,4]{0,1:T(4,128)}, u32[]{:S(2)}) copy-start(s32[16,4]{0,1:T(4,128)} %param.47) | copy-start | bytes 772
  33.6 24.7 %copy-start.2 = (bf16[1,1024,256]{2,1,0:T(8,128)(2,1)S(1)}, bf16[1,1024,256]{2,1,0:T(8,128)(2,1)}, u32[]{:S(2)}) copy-start(bf16[1,1024,256]{2,1,0:T(8,128)(2,1)} %param.49) | copy-start | bytes 1572868
  37.1 70.2 %copy-start.7 = (bf16[1024]{0:T(1024)(128)(2,1)S(1)}, bf16[1024]{0:T(1024)(128)(2,1)}, u32[]{:S(2)}) copy-start(bf16[1024]{0:T(1024)(128)(2,1)} %param.55) | copy-start | bytes 6148
  37.1 70.2 %copy-start.3 = (f32[16,4]{0,1:T(4,128)S(1)}, f32[16,4]{0,1:T(4,128)}, u32[]{:S(2)}) copy-start(f32[16,4]{0,1:T(4,128)} %param.48) | copy-start | bytes 772
  37.1 70.8 %copy-start.8 = (bf16[1024]{0:T(1024)(128)(2,1)S(1)}, bf16[1024]{0:T(1024)(128)(2,1)}, u32[]{:S(2)}) copy-start(bf16[1024]{0:T(1024)(128)(2,1)} %param.59) | copy-start | bytes 6148
  61.2 120.6 %reduce-scatter.5.cloned.1.call-start = ((), (), s32[]{:S(2)}) async-start(), calls=%async_computation.8 | async-start | bytes 1114112 | tf_op jit(solution)/shard_map/reduce_scatter | solution.py:221
  109.7 12.0 %all-to-all-start.1 = ((bf16[16,1,6,1024]{3,2,1,0:T(8,128)(2,1)}), bf16[16,1,6,1024]{3,2,1,0:T(8,128)(2,1)S(1)}, u32[]{:S(2)}, u32[]{:S(2)}) async-start(bf16[16,1,6,1024]{3,2,1,0:T(8,128)(2,1)} %copy.81), calls=%async_computation.2 | async-start | bytes 524288 | tf_op jit(solution)/shard_map/all_to_all | solution.py:207
Sparse Core Ops, SparseCore 0:
  9.5 11.5 all-gather.3
  22.7 10.1 all-gather.7
  34.4 9.9 all-gather.5
  61.4 5.7 reduce-scatter.2
  107.3 74.5 reduce-scatter.4
where the time goes:
time: 192 us; the launch traced here: 191 us
  waiting for transfers between devices  69 us (36%)
  blocking collectives  61.1 us (32%)
  matrix products  29.1 us (15%)
  between operations  14.1 us (7%)
  other arithmetic  7.47 us (4%)
  local copies, waits for them, and re-layouts  6.79 us (4%)
  starting transfers between devices  3.72 us (2%)
    reduce_scatter x1, waiting for transfers between devices, shards(): lax.psum_scatter(dense_partial(rows_side, chip_gate, chip_up, chip_down),...  59.9 us
    all_gather x1, blocking collectives, shards(): rows_side = lax.all_gather(moe_in, 'ep', axis=0, tiled=True)  40.8 us
    all_to_all x1, blocking collectives, shards(): lax.all_to_all(outgoing, 'ep', split_axis=0, concat_axis=0, tiled=True)  18.2 us
    all_to_all x1, waiting for transfers between devices, shards(): lax.all_to_all(summed.astype(jnp.bfloat16), 'ep', split_axis=0, concat_ax...  6.87 us
    dot_general x1, matrix products, attention(): jnp.einsum('shc,slc->shl', query_lat, latent, preferred_element_type=f32)  6.1 us
  transfers between devices with their start and end apart: 6, of which 2 were waited for; matrix products, arithmetic and copies ran while one was open for 21% of the time, Pallas kernels for 0%

commit v1 on v0

v1 whole, which is shorter than its diff:
```python
import functools

import jax
import jax.numpy as jnp
from jax import lax
from jax.experimental import pallas as pl
from jax.experimental.pallas import tpu as pltpu
from jax.sharding import PartitionSpec as P

HEADS = 16
NOPE = 64
ROPE = 32
VDIM = 64


eps = 1e-06
rope_base = 10000.0
routed_scale = 2.5


def rms_scale(value, gain):
    value = value.astype(jnp.float32)
    inverse = lax.rsqrt(jnp.mean(value * value, axis=-1, keepdims=True) + eps)
    return value * inverse * gain.astype(jnp.float32)


def angles(lengths, rope_dim):
    half = rope_dim // 2
    freqs = rope_base ** (-jnp.arange(half, dtype=jnp.float32) / half)
    angle = lengths.astype(jnp.float32)[:, None] * freqs[None, :]
    return (jnp.cos(angle), jnp.sin(angle))


def attention_kernel(
    batch,
    experts,
    lens_ref,
    tokens_ref,
    cos_ref,
    sin_ref,
    meta_ref,
    attn_gain,
    q_gain,
    kv_gain,
    post_gain,
    moe_gain,
    dense_vec,
    *refs,
):
    f32, bf16 = jnp.float32, jnp.bfloat16
    hbm, (first_ref, x_ref, latent_out), bufs = refs[:10], refs[10:13], refs[13:23]
    query, spun, mixed, sem, cache_sem = refs[23:]
    w_dq, w_dkv, w_krope, w_q_nope, w_q_rope, w_uk, latent, rope, w_uv, w_o = bufs
    seqs, length, wide = latent.shape
    width = tokens_ref.shape[1]

    weights = [0, 1, 2, 3, 4, 5, 8, 9]
    loads = {i: pltpu.make_async_copy(hbm[i], bufs[i], sem.at[i]) for i in weights}

    def cache_load(s):
        return (
            pltpu.make_async_copy(hbm[6].at[s], latent.at[s], cache_sem.at[0, s]),
            pltpu.make_async_copy(hbm[7].at[s], rope.at[s], cache_sem.at[1, s]),
        )

    for i in weights[:6]:
        loads[i].start()

    @pl.loop(0, seqs)
    def _(s):
        for load in cache_load(s):
            load.start()

    for i in weights[6:]:
        loads[i].start()

    def mul(a, b):
        return jnp.dot(a, b, preferred_element_type=f32)

    def mul_t(a, b):
        return lax.dot_general(a, b, (((1,), (1,)), ((), ())), preferred_element_type=f32)

    tokens = tokens_ref[...].astype(f32)
    normed = rms_scale(tokens, attn_gain[...]).astype(bf16)
    loads[0].wait()
    q_normed = rms_scale(mul(normed, w_dq[...]), q_gain[...]).astype(bf16)
    loads[1].wait()
    new_latent = rms_scale(mul(normed, w_dkv[...]), kv_gain[...]).astype(bf16)
    latent_out[...] = new_latent
    fresh = new_latent.astype(f32)
    loads[2].wait()
    half = ROPE // 2
    raw = mul(normed, w_krope[...])
    swapped = jnp.concatenate([raw[:, half:], raw[:, :half]], axis=1)
    new_rope = (raw * cos_ref[:, :ROPE] + swapped * sin_ref[:, :ROPE]).astype(bf16).astype(f32)
    loads[3].wait()
    q_nope = mul(q_normed, w_q_nope[...]).astype(bf16)
    loads[4].wait()
    raw = mul(q_normed, w_q_rope[...])
    span = raw.shape[1]
    lane = lax.broadcasted_iota(jnp.int32, raw.shape, 1)
    swapped = jnp.where(
        lane % ROPE < half, pltpu.roll(raw, span - half, 1), pltpu.roll(raw, half, 1)
    )
    q_rot = (raw * cos_ref[...] + swapped * sin_ref[...]).astype(bf16).astype(f32)
    for h in range(HEADS):
        spun[:, h, :] = q_rot[:, h * ROPE : (h + 1) * ROPE]
    loads[5].wait()
    low = lax.broadcasted_iota(jnp.int32, (seqs, 2 * NOPE), 1) < NOPE
    for pair in range(HEADS // 2):
        at = slice(pair * 2 * NOPE, (pair + 1) * 2 * NOPE)
        both = q_nope[:, at].astype(f32)
        both = jnp.concatenate([jnp.where(low, both, 0.0), jnp.where(low, 0.0, both)], axis=0)
        lat = mul_t(both.astype(bf16), w_uk[:, at]).astype(bf16).astype(f32)
        query[:, 2 * pair, :] = lat[:seqs]
        query[:, 2 * pair + 1, :] = lat[seqs:]

    scale = (NOPE + ROPE) ** (-0.5)
    place = lax.broadcasted_iota(jnp.int32, (HEADS, length), 1)
    row = lax.broadcasted_iota(jnp.int32, (seqs, 1), 0)

    @pl.loop(0, seqs // batch)
    def _(step):
        ids = [step * batch + i for i in range(batch)]
        for s in ids:
            for load in cache_load(s):
                load.wait()
        for s in ids:
            mine, turned, keys = query[s], spun[s], latent[s]
            own_key = jnp.sum(jnp.where(row == s, fresh, 0.0), axis=0, keepdims=True)
            own_rope = jnp.sum(jnp.where(row == s, new_rope, 0.0), axis=0, keepdims=True)
            past = (mul_t(mine.astype(bf16), keys) + mul(turned.astype(bf16), rope[s])) * scale
            own = jnp.sum(mine * own_key, axis=1, keepdims=True)
            own = (own + jnp.sum(turned * own_rope, axis=1, keepdims=True)) * scale
            valid = place < lens_ref[s]
            top = jnp.max(jnp.where(valid, past, -1e30), axis=1, keepdims=True)
            top = jnp.maximum(top, own)
            past = jnp.where(valid, jnp.exp(past - top), 0.0)
            own = jnp.exp(own - top)
            total = jnp.sum(past, axis=1, keepdims=True) + own
            out = mul((past / total).astype(bf16), keys)
            mixed[s] = out + (own / total).astype(bf16).astype(f32) * own_key

    loads[8].wait()
    parts = []
    for pair in range(HEADS // 2):
        at = slice(pair * 2 * VDIM, (pair + 1) * 2 * VDIM)
        both = jnp.concatenate([mixed[:, 2 * pair, :], mixed[:, 2 * pair + 1, :]], axis=0)
        both = mul(both.astype(bf16), w_uv[:, at])
        lane = lax.broadcasted_iota(jnp.int32, (seqs, 2 * VDIM), 1)
        parts.append(jnp.where(lane < VDIM, both[:seqs], both[seqs:]))
    head_out = jnp.concatenate(parts, axis=1).astype(bf16)
    loads[9].wait()
    first = (tokens + rms_scale(mul(head_out, w_o[...]), post_gain[...])).astype(bf16)
    first_ref[...] = first
    moe_in = rms_scale(first, moe_gain[...]).astype(bf16)
    x_ref[:, :width] = moe_in
    gate = jnp.sum(moe_in.astype(f32) * dense_vec[...].astype(f32), axis=1, keepdims=True)
    gate = jax.nn.sigmoid(gate)
    lane = lax.broadcasted_iota(jnp.int32, meta_ref.shape, 1)
    columns = experts + 1
    rest = jnp.where(lane % columns == experts, gate, meta_ref[...])
    out = jnp.zeros_like(rest)
    for part in range(PARTS):
        piece = rest.astype(bf16).astype(f32)
        here = (lane >= part * columns) & (lane < (part + 1) * columns)
        out = jnp.where(here, piece, out)
        rest = rest - piece
    x_ref[:, width:] = out.astype(bf16)


def attention(tokens, lengths, meta, experts, gains, big):
    f32, bf16 = jnp.float32, jnp.bfloat16
    seqs, width = tokens.shape
    cosine, sine = angles(lengths, ROPE)
    cosine = jnp.tile(jnp.concatenate([cosine, cosine], axis=1), (1, HEADS))
    sine = jnp.tile(jnp.concatenate([-sine, sine], axis=1), (1, HEADS))
    wide = big[6].shape[2]
    batch = 4 if seqs % 4 == 0 else 1
    vmem = pl.BlockSpec(memory_space=pltpu.VMEM)
    return pl.pallas_call(
        functools.partial(attention_kernel, batch, experts),
        out_shape=(
            jax.ShapeDtypeStruct((seqs, width), bf16),
            jax.ShapeDtypeStruct((seqs, width + meta.shape[1]), bf16),
            jax.ShapeDtypeStruct((seqs, wide), bf16),
        ),
        in_specs=[pl.BlockSpec(memory_space=pltpu.SMEM)]
        + [vmem] * 10
        + [pl.BlockSpec(memory_space=pltpu.HBM)] * 10,
        out_specs=(vmem, vmem, vmem),
        scratch_shapes=[pltpu.VMEM(w.shape, w.dtype) for w in big]
        + [
            pltpu.VMEM((seqs, HEADS, wide), f32),
            pltpu.VMEM((seqs, HEADS, ROPE), f32),
            pltpu.VMEM((seqs, HEADS, wide), f32),
            pltpu.SemaphoreType.DMA((10,)),
            pltpu.SemaphoreType.DMA((2, seqs)),
        ],

        name="attention",
    )(lengths, tokens, cosine, sine, meta, *[g.reshape(1, -1) for g in gains], *big)


MESH = pl.DeviceIdType.MESH
PARTS = 3


def partner(me, k, count):
    other, bit = me, 1
    while bit < count:
        other = other + bit * ((k // bit) % 2) * (1 - 2 * ((me // bit) % 2))
        bit *= 2
    return other


def meta_width(experts):
    return -(-PARTS * (experts + 1) // 128) * 128


def exchange_kernel(
    count,
    groups,
    x_ref,
    first_ref,
    gain_ref,
    eg_hbm,
    eu_hbm,
    ed_hbm,
    dg_hbm,
    du_hbm,
    dd_hbm,
    sg_hbm,
    su_hbm,
    sd_hbm,
    out_ref,
    eg,
    eu,
    ed,
    dg,
    du,
    dd,
    sg,
    su,
    sd,
    rows,
    keep,
    to_sib,
    from_sib,
    to_home,
    from_home,
    load_sem,
    row_send,
    row_recv,
    relay_send,
    relay_recv,
    sib_send,
    sib_recv,
    home_send,
    home_recv,
):
    f32, bf16 = jnp.float32, jnp.bfloat16
    seqs, wide = x_ref.shape
    width = first_ref.shape[1]
    me = lax.axis_index("ep")
    core = lax.axis_index("tp")
    sibling = (me, 1 - core)
    size = count // groups

    loads = [
        pltpu.make_async_copy(src, dst, load_sem.at[i])
        for i, (src, dst) in enumerate(
            (
                (sg_hbm, sg),
                (su_hbm, su),
                (sd_hbm, sd),
                (eg_hbm.at[0], eg),
                (eu_hbm.at[0], eu),
                (dg_hbm, dg),
                (du_hbm, du),
                (ed_hbm.at[0], ed),
                (dd_hbm, dd),
            )
        )
    ]
    for load in loads:
        load.start()

    barrier = pltpu.get_barrier_semaphore()
    pl.semaphore_signal(barrier, inc=1, device_id=sibling, device_id_type=MESH)

    @pl.loop(1, count)
    def _(k):
        pl.semaphore_signal(
            barrier, inc=1, device_id=(partner(me, k, count), core), device_id_type=MESH
        )

    pl.semaphore_wait(barrier, count)

    def row_copy(k, src, hop):
        return pltpu.make_async_remote_copy(
            src_ref=src,
            dst_ref=rows.at[0, k],
            send_sem=row_send.at[k],
            recv_sem=row_recv.at[k],
            device_id=(partner(me, hop, count), core),
            device_id_type=MESH,
        )

    def relay_copy(k, src):
        return pltpu.make_async_remote_copy(
            src_ref=src,
            dst_ref=rows.at[1, k],
            send_sem=relay_send.at[k],
            recv_sem=relay_recv.at[k],
            device_id=sibling,
            device_id_type=MESH,
        )

    def sib_copy(g):
        return pltpu.make_async_remote_copy(
            src_ref=to_sib.at[pl.ds(g * size, size)],
            dst_ref=from_sib.at[pl.ds(g * size, size)],
            send_sem=sib_send.at[g],
            recv_sem=sib_recv.at[g],
            device_id=sibling,
            device_id_type=MESH,
        )

    def home_copy(k, hop):
        return pltpu.make_async_remote_copy(
            src_ref=to_home.at[k],
            dst_ref=from_home.at[k],
            send_sem=home_send.at[k],
            recv_sem=home_recv.at[k],
            device_id=(partner(me, hop, count), core),
            device_id_type=MESH,
        )

    for g in range(1, groups):
        row_copy(g * size, x_ref, g * size).start()

    @pl.loop(1, size)
    def _(m):
        row_copy(m, x_ref, m).start()

    relay_copy(0, x_ref).start()
    own = pltpu.make_async_copy(x_ref, rows.at[0, 0], row_recv.at[0])
    own.start()

    for load in loads[:3]:
        load.wait()
    mine = x_ref[:, :width]
    hidden = (
        jax.nn.silu(jnp.dot(mine, sg[...], preferred_element_type=f32))
        * jnp.dot(mine, su[...], preferred_element_type=f32)
    ).astype(bf16)
    total = jnp.dot(hidden, sd[...], preferred_element_type=f32)
    for g in range(1, groups):
        row_copy(g * size, x_ref, g * size).wait_recv()

        @pl.loop(1, size)
        def _(m):
            row_copy(g * size + m, rows.at[0, g * size], m).start()

    for load in loads[3:]:
        load.wait()
    own.wait()

    lane = lax.broadcasted_iota(jnp.int32, (1, wide - width), 1)
    columns = count + 1

    def picked(meta, column):
        chosen = lane == column
        for part in range(1, PARTS):
            chosen = chosen | (lane == column + part * columns)
        return jnp.sum(jnp.where(chosen, meta, 0.0), axis=1, keepdims=True)

    def send_home(g):
        sib_copy(g).wait_recv()
        part = keep[g * size : (g + 1) * size] + from_sib[g * size : (g + 1) * size].astype(f32)
        to_home[g * size : (g + 1) * size] = part.astype(bf16)

        keep[g * size] = part[0]

        @pl.loop(1, size)
        def _(m):
            home_copy(g * size + m, m).start()

    def plane_sum(g):
        @pl.loop(1, size)
        def _(m):
            home_copy(g * size + m, m).wait_recv()

        part = keep[g * size]
        for m in range(1, size):
            part = part + from_home[g * size + m].astype(f32)
        return part

    def send_far(g):
        to_home[g * size] = plane_sum(g).astype(bf16)
        home_copy(g * size, g * size).start()

    order = list(range(1, groups)) + [0]
    for turn, g in enumerate(order):
        if g > 0:
            relay_copy(g * size, rows.at[0, g * size]).start()

        @pl.loop(g * size + 1, (g + 1) * size)
        def _(k):
            row_copy(k, x_ref, 1).wait_recv()
            relay_copy(k, rows.at[0, k]).start()

        if turn > 0:
            send_home(order[turn - 1])

        @pl.loop(g * size, (g + 1) * size)
        def _(k):
            relay_copy(k, x_ref).wait_recv()

        block = rows[:, g * size : (g + 1) * size].reshape(2 * size * seqs, wide)
        values, meta = block[:, :width], block[:, width:].astype(f32)
        act = (
            jax.nn.silu(jnp.dot(values, eg[...], preferred_element_type=f32))
            * jnp.dot(values, eu[...], preferred_element_type=f32)
        ).astype(bf16)
        routed = jnp.dot(act, ed[...], preferred_element_type=f32).astype(bf16).astype(f32)
        act = (
            jax.nn.silu(jnp.dot(values, dg[...], preferred_element_type=f32))
            * jnp.dot(values, du[...], preferred_element_type=f32)
        ).astype(bf16)
        dense = jnp.dot(act, dd[...], preferred_element_type=f32)
        part = routed * picked(meta, me) + dense * picked(meta, count)
        part = part.reshape(2, size, seqs, width)
        to_sib[g * size : (g + 1) * size] = part[1].astype(bf16)
        sib_copy(g).start()
        keep[g * size : (g + 1) * size] = part[0]

    send_home(order[-1])
    for g in range(1, groups):
        send_far(g)
    total = total + plane_sum(0)
    for g in range(1, groups):
        home_copy(g * size, g * size).wait_recv()
        total = total + from_home[g * size].astype(f32)
    inverse = lax.rsqrt(jnp.mean(total * total, axis=-1, keepdims=True) + eps)
    out_ref[...] = (
        first_ref[...].astype(f32) + total * inverse * gain_ref[...].astype(f32)
    ).astype(bf16)

    relay_copy(0, x_ref).wait_send()

    @pl.loop(1, count)
    def _(k):
        row_copy(k, x_ref, 1).wait_send()
        relay_copy(k, rows.at[0, k]).wait_send()
        home_copy(k, 1).wait_send()

    for g in range(groups):
        sib_copy(g).wait_send()


def exchange(rows, first, gain, expert, dense, shared):
    bf16, f32 = jnp.bfloat16, jnp.float32
    count = lax.axis_size("ep")
    groups = min(4, count)
    seqs, width = first.shape
    wide = rows.shape[1]
    any_space = pl.BlockSpec(memory_space=pltpu.HBM)
    vmem = pl.BlockSpec(memory_space=pltpu.VMEM)
    dma = pltpu.SemaphoreType.DMA
    weights = list(expert) + list(dense) + list(shared)
    return pl.pallas_call(
        functools.partial(exchange_kernel, count, groups),
        out_shape=jax.ShapeDtypeStruct((seqs, width), bf16),
        in_specs=[vmem] * 3 + [any_space] * 9,
        out_specs=vmem,
        scratch_shapes=[pltpu.VMEM(w.shape[-2:], w.dtype) for w in weights]
        + [
            pltpu.VMEM((2, count, seqs, wide), bf16),
            pltpu.VMEM((count, seqs, width), f32),
            pltpu.VMEM((count, seqs, width), bf16),
            pltpu.VMEM((count, seqs, width), bf16),
            pltpu.VMEM((count, seqs, width), bf16),
            pltpu.VMEM((count, seqs, width), bf16),
            dma((9,)),
            dma((count,)),
            dma((count,)),
            dma((count,)),
            dma((count,)),
            dma((groups,)),
            dma((groups,)),
            dma((count,)),
            dma((count,)),
        ],
        compiler_params=pltpu.CompilerParams(
            collective_id=0, has_side_effects=True
        ),
        name="exchange",
    )(rows, first, gain.reshape(1, width), *weights)


def meta_columns(routes, scores, experts):
    norm = scores / jnp.sum(scores, axis=1, keepdims=True) * routed_scale
    lane = jnp.arange(meta_width(experts), dtype=jnp.int32) % (experts + 1)
    named = routes[:, :, None] == lane[None, None, :]
    return jnp.sum(jnp.where(named, norm[:, :, None], 0.0), axis=1)


def shards(
    tokens,
    lengths,
    cache_latent,
    cache_rope,
    attn_gain,
    w_dq,
    q_gain,
    w_q_nope,
    w_q_rope,
    w_dkv,
    kv_gain,
    w_krope,
    w_uk,
    w_uv,
    w_o,
    post_gain,
    moe_gain,
    routes,
    route_scores,
    expert_gate,
    expert_up,
    expert_down,
    shared_gate,
    shared_up,
    shared_down,
    dense_vec,
    dense_w_gate,
    dense_w_up,
    dense_w_down,
    out_gain,
):
    experts = expert_gate.shape[0] * lax.axis_size("ep")
    first, rows, new_latent = attention(
        tokens,
        lengths,
        meta_columns(routes, route_scores, experts),
        experts,
        (attn_gain, q_gain, kv_gain, post_gain, moe_gain, dense_vec),
        (w_dq, w_dkv, w_krope, w_q_nope, w_q_rope, w_uk, cache_latent, cache_rope, w_uv, w_o),
    )
    hidden_out = exchange(
        rows,
        first,
        out_gain,
        (expert_gate, expert_up, expert_down),
        (dense_w_gate, dense_w_up, dense_w_down),
        (shared_gate, shared_up, shared_down),
    )
    return (hidden_out, new_latent)


def solution(mesh):
    return jax.shard_map(
        shards,
        mesh=mesh,
        in_specs=(
            P(("ep", "tp"), None),
            P(("ep", "tp")),
            P(("ep", "tp"), None, None),
            P(("ep", "tp"), None, None),
            P(),
            P(),
            P(),
            P(),
            P(),
            P(),
            P(),
            P(),
            P(),
            P(),
            P(),
            P(),
            P(),
            P(("ep", "tp"), None),
            P(("ep", "tp"), None),
            P("ep", None, "tp"),
            P("ep", None, "tp"),
            P("ep", "tp", None),
            P(),
            P(),
            P(),
            P(),
            P(None, ("ep", "tp")),
            P(None, ("ep", "tp")),
            P(("ep", "tp"), None),
            P(),
        ),
        out_specs=(P(("ep", "tp"), None), P(("ep", "tp"), None)),
        check_vma=False,
    )
```

time: 192 us -> 63.7 us (0.33)
  waiting for transfers between devices: 69 us -> 0 us
  blocking collectives: 61.1 us -> 0 us
  Pallas kernels: 0 us -> 46.1 us
  matrix products: 29.1 us -> 0 us
  between operations: 14.1 us -> 0.67 us
  local copies, waits for them, and re-layouts: 6.79 us -> 12.7 us
  other arithmetic: 7.47 us -> 3.63 us
  starting transfers between devices: 3.72 us -> 0 us
    reduce_scatter x2 -> x0, waiting for transfers between devices: 60 us -> none  [the longest x1 59.9 us: shards(): lax.psum_scatter(dense_partial(rows_side, chip_gate, chip_up, chip_down),...]
    pallas_call x0 -> x2, Pallas kernels: none -> 46.1 us  [the longest x1 30.7 us: exchange(): pl.pallas_call(functools.partial(exchange_kernel, count, groups), out_sha...]
    all_gather x2 -> x0, blocking collectives: 42.9 us -> none  [the longest x1 40.8 us: shards(): rows_side = lax.all_gather(moe_in, 'ep', axis=0, tiled=True)]
    dot_general x21 -> x0, matrix products: 29.1 us -> none  [the longest x1 6.1 us: attention(): jnp.einsum('shc,slc->shl', query_lat, latent, preferred_element_type=f32)]
    all_to_all x1 -> x0, blocking collectives: 18.2 us -> none  [shards(): lax.all_to_all(outgoing, 'ep', split_axis=0, concat_axis=0, tiled=True)]
    reshape x5 -> x7, local copies, waits for them, and re-layouts: 0.47 us -> 8.2 us  [the longest x6 7.6 us: attention(): g.reshape(1, -1)]
    all_to_all x1 -> x0, waiting for transfers between devices: 6.87 us -> none  [shards(): lax.all_to_all(summed.astype(jnp.bfloat16), 'ep', split_axis=0, concat_ax...]
    convert_element_type x11 -> x0, other arithmetic: 3.83 us -> none  [the longest x6 2.88 us: rms_scale(): return value * inverse * gain.astype(jnp.float32)]
  transfers between devices with their start and end apart: 6 -> 0, of which waited for: 2 -> 0; matrix products, arithmetic and copies ran while one was open for 21% -> 0% of each run, Pallas kernels for 0% -> 0%
where the time goes in v1:
time: 63.7 us; the launch traced here: 63.2 us
  Pallas kernels  46.1 us (72%)
  local copies, waits for them, and re-layouts  12.7 us (20%)
  other arithmetic  3.63 us (6%)
  between operations  0.67 us (1%)
    pallas_call x1, Pallas kernels, exchange(): pl.pallas_call(functools.partial(exchange_kernel, count, groups), out_sha...  30.7 us
    pallas_call x1, Pallas kernels, attention(): pl.pallas_call(functools.partial(attention_kernel, batch, experts), out_s...  15.5 us
    reshape x6, local copies, waits for them, and re-layouts, attention(): g.reshape(1, -1)  7.6 us
    unnamed x4, local copies, waits for them, and re-layouts  3.05 us
    reduce_sum x1, other arithmetic, meta_columns(): return jnp.sum(jnp.where(named, norm[:, :, None], 0.0), axis=1)  1.37 us

profile of v1, /device:TPU:0, one launch (start us, length us, event | category | flops | bytes accessed | tf_op | source)
XLA Modules:
  0.0 63.2 jit_solution(15578773098031059709)
XLA Ops:
  0.6 0.7 %convert_element_type.3 = f32[16]{0:T(128)S(1)} convert(s32[16]{0:T(128)} %lens_ref.1) | non-fusion elementwise | flops 16 | bytes 128 | tf_op jit(solution)/shard_map/convert_element_type | solution.py:30
  1.3 0.1 fusion
  1.4 0.1 pad_maximum_fusion
  1.5 0.7 %tile.21.sin_ref = f32[16,512]{1,0:T(8,128)} reshape(f32[16,16,32]{2,1,0:T(8,128)S(1)} %tile.20) | data formatting | bytes 65536 | tf_op jit(solution)/shard_map/tile | solution.py:177
  2.2 0.0 copy-start
  2.2 0.7 %tile.9.cos_ref = f32[16,512]{1,0:T(8,128)} reshape(f32[16,16,32]{2,1,0:T(8,128)S(1)} %tile.8) | data formatting | bytes 65536 | tf_op jit(solution)/shard_map/tile | solution.py:176
  3.0 1.7 %copy.35.refs_2_ = bf16[1024,32]{1,0:T(8,128)(2,1)} copy(bf16[1024,32]{0,1:T(8,128)(2,1)} %param.41) | data formatting | bytes 131072 | tf_op args[11]
  4.6 0.7 %reduce_sum.18 = f32[16]{0:T(128)S(1)} reduce(f32[16,4]{0,1:T(4,128)} %param.48, f32[]{:T(128)} %constant.19.clone.1), dimensions={1}, to_apply=%region_0.0 | reduce | flops 48 | bytes 324 | tf_op jit(solution)/shard_map/reduce_sum | solution.py:504
  5.3 0.7 %divide_multiply_fusion = f32[16,4]{0,1:T(4,128)S(1)} fusion(f32[16,4]{0,1:T(4,128)} %param.48, f32[16]{0:T(128)S(1)} %reduce_sum.18), kind=kLoop, calls=%fused_computation.6 | loop fusion | flops 128 | bytes 576 | tf_op jit(solution)/shard_map/mul | solution.py:504
  6.0 1.4 %select_reduce_fusion.meta_ref = f32[16,128]{1,0:T(8,128)} fusion(f32[16,4]{0,1:T(4,128)S(1)} %divide_multiply_fusion, s32[128]{0:T(128)S(1)} %and_select_fusion, s32[16,4]{0,1:T(4,128)} %param.47), kind=kLoop, calls=%fused_computation | loop fusion | flops 22528 | bytes 9216 | tf_op jit(solution)/shard_map/reduce_sum | solution.py:507
  7.4 1.3 %reshape.52.attn_gain = bf16[1,1024]{1,0:T(2,128)(2,1)} reshape(bf16[1024]{0:T(1024)(128)(2,1)} %param.34) | data formatting | bytes 4096 | tf_op jit(solution)/shard_map/reshape | solution.py:202
  8.7 1.3 %reshape.55.post_gain = bf16[1,1024]{1,0:T(2,128)(2,1)} reshape(bf16[1024]{0:T(1024)(128)(2,1)} %param.45) | data formatting | bytes 4096 | tf_op jit(solution)/shard_map/reshape | solution.py:202
  9.9 1.3 %reshape.56.moe_gain = bf16[1,1024]{1,0:T(2,128)(2,1)} reshape(bf16[1024]{0:T(1024)(128)(2,1)} %param.46) | data formatting | bytes 4096 | tf_op jit(solution)/shard_map/reshape | solution.py:202
  11.2 1.3 %reshape.57.dense_vec = bf16[1,1024]{1,0:T(2,128)(2,1)} reshape(bf16[1024]{0:T(1024)(128)(2,1)} %param.55) | data formatting | bytes 4096 | tf_op jit(solution)/shard_map/reshape | solution.py:202
  12.5 1.3 %reshape.53.q_gain = bf16[1,512]{1,0:T(2,128)(2,1)} reshape(bf16[512]{0:T(512)(128)(2,1)} %param.36) | data formatting | bytes 2048 | tf_op jit(solution)/shard_map/reshape | solution.py:202
  13.8 1.2 %reshape.54.kv_gain = bf16[1,256]{1,0:T(2,128)(2,1)} reshape(bf16[256]{0:T(256)(128)(2,1)} %param.40) | data formatting | bytes 1024 | tf_op jit(solution)/shard_map/reshape | solution.py:202
  15.0 15.5 %attention.1 = (bf16[16,1024]{1,0:T(8,128)(2,1)}, bf16[16,1152]{1,0:T(8,128)(2,1)}, bf16[16,256]{1,0:T(8,128)(2,1)}) custom-call(s32[16]{0:T(128)} %lens_ref.1, bf16[16,1024]{1,0:T(8,128)(2,1)} %tokens_ref.1, f32[16,512]{1,0:T(8,128)} %tile.9.cos_ref, f32[16,512]{1,0:T(8,128)} %tile.21.sin_ref, f32[16,128]{1,0:T(8,128)} %select_reduce_fusion.meta_ref, ...), custom_call_target="tpu_custom_call" | custom-call | tf_op jit(solution)/shard_map/attention/pallas_call | solution.py:181
  30.5 0.0 copy-done
  30.5 0.6 reshape.58.gain_ref
  31.1 30.7 %exchange.1 = bf16[16,1024]{1,0:T(8,128)(2,1)} custom-call(bf16[16,1152]{1,0:T(8,128)(2,1)} %get-tuple-element.5.x_ref, bf16[16,1024]{1,0:T(8,128)(2,1)} %get-tuple-element.6.first_ref, bf16[1,1024]{1,0:T(2,128)(2,1)} %reshape.58.gain_ref, bf16[1,1024,256]{2,1,0:T(8,128)(2,1)} %eg_hbm.1, bf16[1,1024,256]{2,1,0:T(8,128)(2,1)} %eu_hbm.1, ...), custom_call_target="tpu_custom_call" | custom-call | tf_op jit(solution)/shard_map/exchange/pallas_call | solution.py:473
  61.8 1.4 %copy.37 = bf16[16,1024]{1,0:T(8,128)(2,1)} copy(bf16[16,1024]{1,0:T(8,128)(2,1)} %exchange.1) | data formatting | bytes 65536
  (4 shorter events, 0.0 us)
Async XLA Ops:
  2.2 28.3 %copy-start = (bf16[1024]{0:T(1024)(128)(2,1)S(1)}, bf16[1024]{0:T(1024)(128)(2,1)}, u32[]{:S(2)}) copy-start(bf16[1024]{0:T(1024)(128)(2,1)} %param.59) | copy-start | bytes 6148
